TPU v7x, 32 devices: a whole 2x2x4 slice. The times are simulated.
32 devices in a mesh: ep: 16 (over z, x, core), tp: 2 (over y).
Axes of the slice: x: 2, y: 2, z: 4, core: 2. Of those that a mesh axis runs over, the one named last changes fastest.
Arguments:
- tokens: bfloat16 [2048, 2048], P('ep'), may hold values from -6 to 6
- routes: int32 [2048, 2], P('ep'), may hold values from 0 to 3, all different within a row; in each aligned block of 128 rows (0 to 127, 128 to 255, ...) at most 80 rows name the same one
- router_weight: bfloat16 [2048, 4], replicated, may hold values from -0.125 to 0.125
- gate_proj: bfloat16 [16, 2048, 1024], P('ep', None, 'tp'), may hold values from -0.125 to 0.125
- up_proj: bfloat16 [16, 2048, 1024], P('ep', None, 'tp'), may hold values from -0.125 to 0.125
- down_proj: bfloat16 [16, 1024, 2048], P('ep', 'tp'), may hold values from -0.09375 to 0.09375
- cotangent: bfloat16 [2048, 2048], P('ep'), may hold values from -1.5 to 1.5
Outputs:
- token_grad: bfloat16 [2048, 2048], P('ep', 'tp')
- gate_grad: float32 [2048, 2], P('ep')
- router_grad: float32 [2048, 4], P('ep')
- gate_proj_grad: float32 [16, 2048, 1024], P('ep', None, 'tp')
- up_proj_grad: float32 [16, 2048, 1024], P('ep', None, 'tp')
- down_proj_grad: float32 [16, 1024, 2048], P('ep', 'tp')
Inputs may be any that keep to these rules, and one draw needn't show every extreme that they name: `routes`: each row names 2 different experts. Among the rows of one index of ep no expert is named more than 80 times, a bound that some block reaches.
All inputs are finite; a program needn't handle non-finite values.
Results may differ from a plain program's by a relative error of at most 0.0085.
Values may be sent and summed in bfloat16 or wider, within the bound.
No kernel may reach another device: no remote copies, remote signals or barrier semaphores. Data moves between devices by JAX's collectives and lax.ppermute only.
A program may use at most 128 MiB of HBM per device.

v0:
```python
import jax
import jax.numpy as jnp
from jax import lax
from jax.sharding import PartitionSpec as P

MEMBERS = 4
TOP = 2


def shards(tokens, routes, router_weight, gate_proj, up_proj, down_proj, cotangent):
    ntok = tokens.shape[0]
    width = tokens.shape[1]
    experts = router_weight.shape[1]
    n_ep = lax.axis_size("ep")
    n_tp = lax.axis_size("tp")
    share = width // n_tp
    capacity = min(ntok, 5 * TOP * ntok // (4 * experts))
    tp_index = lax.axis_index("tp")
    logits = jnp.dot(tokens, router_weight, preferred_element_type=jnp.float32)
    onehot = (routes[:, :, None] == jnp.arange(experts, dtype=jnp.int32)[None, None, :]).astype(
        jnp.float32
    )
    chosen = jnp.sum(onehot * logits[:, None, :], axis=2)
    first = jax.nn.sigmoid(chosen[:, 0] - chosen[:, 1])
    gates = jnp.stack([first, 1.0 - first], axis=1)
    used = gates.astype(jnp.bfloat16)
    flat = onehot.reshape(ntok * TOP, experts)
    rank = jnp.cumsum(flat, axis=0) - flat
    rank_sel = jnp.sum(flat * rank, axis=1).astype(jnp.int32)
    target = routes.reshape(-1) * capacity + rank_sel
    placing = (jnp.arange(experts * capacity, dtype=jnp.int32)[:, None] == target[None, :]).astype(
        jnp.float32
    )
    place_tok = jnp.sum(placing.reshape(experts * capacity, ntok, TOP), axis=2)
    place_bf = place_tok.astype(jnp.bfloat16)

    def spread(buffer):
        tail = buffer.shape[1:]
        grown = jnp.broadcast_to(
            buffer.reshape((experts, 1, capacity) + tail), (experts, MEMBERS, capacity) + tail
        )
        return grown.reshape((n_ep * capacity,) + tail)

    gate_slots = jnp.dot(
        placing, used.reshape(-1).astype(jnp.float32), precision=lax.Precision.HIGHEST
    ).astype(jnp.bfloat16)
    gate_send = spread(gate_slots[:, None])[:, 0]
    tok_part = lax.dynamic_slice_in_dim(tokens, tp_index * share, share, 1)
    cot_part = lax.dynamic_slice_in_dim(cotangent, tp_index * share, share, 1)
    tok_send = spread(
        jnp.dot(place_bf, tok_part, preferred_element_type=jnp.float32).astype(jnp.bfloat16)
    )
    cot_send = spread(
        jnp.dot(place_bf, cot_part, preferred_element_type=jnp.float32).astype(jnp.bfloat16)
    )
    tok_half, cot_half, gate_rows = (
        lax.all_to_all(tok_send, "ep", split_axis=0, concat_axis=0, tiled=True),
        lax.all_to_all(cot_send, "ep", split_axis=0, concat_axis=0, tiled=True),
        lax.all_to_all(gate_send, "ep", split_axis=0, concat_axis=0, tiled=True),
    )
    tok_rows, cot_rows = (
        lax.all_gather(tok_half, "tp", axis=1, tiled=True),
        lax.all_gather(cot_half, "tp", axis=1, tiled=True),
    )
    w_gate = gate_proj[0]
    w_up = up_proj[0]
    w_down = down_proj[0]
    gpre = jnp.dot(tok_rows, w_gate, preferred_element_type=jnp.float32)
    upre = jnp.dot(tok_rows, w_up, preferred_element_type=jnp.float32)
    sig = jax.nn.sigmoid(gpre)
    silu_val = gpre * sig
    hidden = (silu_val * upre).astype(jnp.bfloat16)
    qvals = lax.dot_general(
        cot_rows, w_down, (((1,), (1,)), ((), ())), preferred_element_type=jnp.float32
    )
    gate_part = jnp.sum(hidden.astype(jnp.float32) * qvals, axis=1)
    weight = gate_rows.astype(jnp.float32)[:, None]
    dhid = weight * qvals
    d_gate = (dhid * upre * sig * (1.0 + gpre * (1.0 - sig))).astype(jnp.bfloat16)
    d_up = (dhid * silu_val).astype(jnp.bfloat16)
    scaled = (weight * hidden.astype(jnp.float32)).astype(jnp.bfloat16)
    grad_down = lax.dot_general(
        scaled, cot_rows, (((0,), (0,)), ((), ())), preferred_element_type=jnp.float32
    )
    grad_gate = lax.dot_general(
        tok_rows, d_gate, (((0,), (0,)), ((), ())), preferred_element_type=jnp.float32
    )
    grad_up = lax.dot_general(
        tok_rows, d_up, (((0,), (0,)), ((), ())), preferred_element_type=jnp.float32
    )
    row_grad = lax.dot_general(
        d_gate, w_gate, (((1,), (1,)), ((), ())), preferred_element_type=jnp.float32
    )
    row_grad = row_grad + lax.dot_general(
        d_up, w_up, (((1,), (1,)), ((), ())), preferred_element_type=jnp.float32
    )
    row_share = lax.psum_scatter(row_grad, "tp", scatter_dimension=1, tiled=True)
    gate_total = lax.psum(gate_part, "tp")
    back_rows, back_gate = (
        lax.all_to_all(row_share, "ep", split_axis=0, concat_axis=0, tiled=True),
        lax.all_to_all(gate_total, "ep", split_axis=0, concat_axis=0, tiled=True),
    )
    back_rows = jnp.sum(back_rows.reshape(experts, MEMBERS, capacity, share), axis=1).reshape(
        experts * capacity, share
    )
    back_gate = jnp.sum(back_gate.reshape(experts, MEMBERS, capacity), axis=1).reshape(
        experts * capacity
    )
    route_sum = lax.dot_general(
        place_tok, back_rows, (((0,), (0,)), ((), ())), precision=lax.Precision.HIGHEST
    )
    gate_grad = lax.dot_general(
        placing, back_gate, (((0,), (0,)), ((), ())), precision=lax.Precision.HIGHEST
    ).reshape(ntok, TOP)
    delta = first * (1.0 - first) * (gate_grad[:, 0] - gate_grad[:, 1])
    dlogits = delta[:, None] * (onehot[:, 0] - onehot[:, 1])
    router_rows = lax.dynamic_slice_in_dim(router_weight, tp_index * share, share, 0).astype(
        jnp.float32
    )
    router_part = lax.dot_general(
        dlogits, router_rows, (((1,), (1,)), ((), ())), precision=lax.Precision.HIGHEST
    )
    token_grad = (route_sum + router_part).astype(jnp.bfloat16)
    columns = tokens.astype(jnp.float32)
    router_grad = lax.psum_scatter(
        lax.dot_general(
            columns, dlogits, (((0,), (0,)), ((), ())), precision=lax.Precision.HIGHEST
        ),
        "ep",
        scatter_dimension=0,
        tiled=True,
    )
    return (token_grad, gate_grad, router_grad, grad_gate[None], grad_up[None], grad_down[None])


def solution(mesh):
    placed = (
        P("ep", None),
        P("ep", None),
        P(),
        P("ep", None, "tp"),
        P("ep", None, "tp"),
        P("ep", "tp", None),
        P("ep", None),
    )
    return jax.shard_map(
        shards,
        mesh=mesh,
        in_specs=placed,
        out_specs=(
            P("ep", "tp"),
            P("ep", None),
            P("ep", None),
            P("ep", None, "tp"),
            P("ep", None, "tp"),
            P("ep", "tp", None),
        ),
        check_vma=False,
    )
```

profile of v0, /device:TPU:11, one launch (start us, length us, event | category | flops | bytes accessed | tf_op | source)
XLA Modules:
  0.0 496.3 jit_solution(1121042243303813282)
XLA Ops:
  8.5 1.2 reduce-window.6
  11.1 1.3 convolution_convert_fusion
  12.8 64.9 %all_to_all.51 = bf16[16,80,1024]{2,1,0:T(8,128)(2,1)} all-to-all(bf16[16,80,1024]{2,1,0:T(8,128)(2,1)S(1)} %bitcast.86), channel_id=1, replica_groups=mesh['ep'=16,'tp'=2] {'ep'}, dimensions={0} | all-to-all | bytes 5242880 | tf_op jit(solution)/shard_map/all_to_all | solution.py:57
  79.4 63.8 %all_to_all.52 = bf16[16,80,1024]{2,1,0:T(8,128)(2,1)} all-to-all(bf16[16,80,1024]{2,1,0:T(8,128)(2,1)S(1)} %bitcast.87), channel_id=1, replica_groups=mesh['ep'=16,'tp'=2] {'ep'}, dimensions={0} | all-to-all | bytes 5242880 | tf_op jit(solution)/shard_map/all_to_all | solution.py:58
  145.1 8.4 %all_to_all.53 = bf16[16,80,1]{1,2,0:T(2,128)(2,1)S(1)} all-to-all(bf16[16,80,1]{1,2,0:T(2,128)(2,1)S(1)} %copy.64), channel_id=1, replica_groups=mesh['ep'=16,'tp'=2] {'ep'}, dimensions={0} | all-to-all | bytes 5120 | tf_op jit(solution)/shard_map/all_to_all | solution.py:59
  153.7 7.8 %fusion.5 = f32[1280,512]{0,1:T(8,128)} fusion(bf16[1280,2048]{1,0:T(8,128)(2,1)} %all-gather.5.cloned.1.call-done, bf16[1,2048,512]{2,1,0:T(8,128)(2,1)S(1)} %copy-done), kind=kOutput, calls=%fused_computation.17 | convolution fusion | flops 2684354560 | bytes 9961472 | tf_op jit(solution)/shard_map/dot_general | solution.py:68
  161.5 4.6 fusion.8
  166.1 49.9 %all-gather.3.cloned.1.call-done = bf16[1280,2048]{1,0:T(8,128)(2,1)} async-done(((bf16[1280,1024]{1,0:T(8,128)(2,1)}), bf16[1280,2048]{1,0:T(8,128)(2,1)}) %all-gather.3.cloned.1.call-update) | async-done | bytes 5242896 | tf_op jit(solution)/shard_map/all_gather | solution.py:63
  216.1 9.6 %fusion = (f32[1280]{0:T(1024)S(1)}, bf16[1280,512]{0,1:T(8,128)(2,1)}, bf16[1280,512]{0,1:T(8,128)(2,1)S(1)}, bf16[1280,512]{0,1:T(8,128)(2,1)S(1)}) fusion(f32[1280,512]{0,1:T(8,128)} %fusion.8, f32[1280,512]{0,1:T(8,128)} %fusion.5, f32[1280]{0:T(1024)S(1)} %reshape.131, bf16[1280,2048]{1,0:T(8,128)(2,1)} %all-gather.3.cloned.1.call-done, ...), kind=kOutput, calls=%fused_computation.7 | convolution fusion | flops 2696805120 | bytes 16525312 | tf_op jit(solution)/shard_map/dot_general | solution.py:73
  225.7 3.2 fusion.3
  228.9 5.6 %convolution_add_fusion = f32[1280,2048]{1,0:T(8,128)} fusion(f32[1280,2048]{1,0:T(8,128)S(1)} %fusion.3, bf16[1280,512]{0,1:T(8,128)(2,1)S(1)} %get-tuple-element.11, bf16[1,2048,512]{2,1,0:T(8,128)(2,1)S(1)} %copy-done.7), kind=kOutput, calls=%fused_computation | convolution fusion | flops 2686976000 | bytes 24379392 | tf_op jit(solution)/shard_map/dot_general | solution.py:94
  234.6 3.8 psum.7
  238.4 11.4 %all_to_all.54 = f32[16,80,1]{1,2,0:T(1,128)S(1)} all-to-all(f32[16,80,1]{1,2,0:T(1,128)S(1)} %bitcast.93), channel_id=1, replica_groups=mesh['ep'=16,'tp'=2] {'ep'}, dimensions={0} | all-to-all | bytes 10240 | tf_op jit(solution)/shard_map/all_to_all | solution.py:101
  249.8 106.8 %reduce-scatter.5.cloned.1.call-done = f32[1280,1024]{1,0:T(8,128)} async-done(((f32[1280,2048]{1,0:T(8,128)}), f32[1280,1024]{1,0:T(8,128)}) %reduce-scatter.5.cloned.1.call-update) | async-done | bytes 5242896 | tf_op jit(solution)/shard_map/reduce_scatter | solution.py:97
  356.6 6.6 %all-to-all-start.3 = ((f32[16,80,1024]{2,1,0:T(8,128)}), f32[16,80,1024]{2,1,0:T(8,128)}, u32[]{:S(2)}, u32[]{:S(2)}) async-start(f32[16,80,1024]{2,1,0:T(8,128)} %bitcast.88), calls=%async_computation.4 | async-start | bytes 10485760 | tf_op jit(solution)/shard_map/all_to_all | solution.py:100
  363.6 7.2 %convolution_bitcast_fusion.2 = f32[1,2048,512]{2,1,0:T(8,128)} fusion(bf16[1280,2048]{1,0:T(8,128)(2,1)} %all-gather.5.cloned.1.call-done, bf16[1280,512]{0,1:T(8,128)(2,1)S(1)} %copy-done.14), kind=kOutput, calls=%fused_computation.6 | convolution fusion | flops 2684354560 | bytes 10747904 | tf_op jit(solution)/shard_map/dot_general | solution.py:85
  370.9 7.2 %convolution_bitcast_fusion.1 = f32[1,2048,512]{2,1,0:T(8,128)} fusion(bf16[1280,2048]{1,0:T(8,128)(2,1)} %all-gather.5.cloned.1.call-done, bf16[1280,512]{0,1:T(8,128)(2,1)S(1)} %get-tuple-element.11), kind=kOutput, calls=%fused_computation.5 | convolution fusion | flops 2684354560 | bytes 10747904 | tf_op jit(solution)/shard_map/dot_general | solution.py:88
  378.1 4.5 convolution_bitcast_fusion
  383.4 1.4 copy.71
  385.3 85.3 %reduce-scatter.7.cloned.1.call-done = f32[128,4]{1,0:T(8,128)} async-done(((f32[2048,4]{1,0:T(8,128)}), f32[128,4]{1,0:T(8,128)}) %reduce-scatter.7.cloned.1.call-update) | async-done | bytes 2064
  470.7 1.5 copy.72
  472.2 12.4 %all-to-all-done.3 = f32[16,80,1024]{2,1,0:T(8,128)} async-done(((f32[16,80,1024]{2,1,0:T(8,128)}), f32[16,80,1024]{2,1,0:T(8,128)}, u32[]{:S(2)}, u32[]{:S(2)}) %all-to-all-start.3) | async-done | bytes 5242912 | tf_op jit(solution)/shard_map/all_to_all | solution.py:100
  484.6 3.3 bitcast_reduce_fusion
  487.9 1.8 fusion.14
  (90 shorter events, 8.4 us)
Async XLA Ops:
  7.2 146.5 %copy-start = (bf16[1,2048,512]{2,1,0:T(8,128)(2,1)S(1)}, bf16[1,2048,512]{2,1,0:T(8,128)(2,1)}, u32[]{:S(2)}) copy-start(bf16[1,2048,512]{2,1,0:T(8,128)(2,1)} %param.10) | copy-start | bytes 6291460
  7.2 146.5 %all-gather.5.cloned.1.call-start = ((), (), s32[]{:S(2)}) async-start(), calls=%async_computation.8 | async-start | bytes 7864320 | tf_op jit(solution)/shard_map/all_gather | solution.py:62
  11.1 66.7 %copy-start.4 = (f32[320,128]{1,0:T(8,128)}, f32[320,128]{1,0:T(8,128)S(1)}, u32[]{:S(2)}) copy-start(f32[320,128]{1,0:T(8,128)S(1)} %convert_reduce_fusion) | copy-start | bytes 491524
  77.7 1.0 copy-start.8
  77.7 138.4 %all-gather.3.cloned.1.call-start = ((), (), s32[]{:S(2)}) async-start(), calls=%async_computation.7 | async-start | bytes 7864320 | tf_op jit(solution)/shard_map/all_gather | solution.py:63
  143.2 1.0 copy-start.2
  143.2 1.0 copy-start.9
  143.2 1.3 copy-start.10
  143.2 213.4 %reduce-scatter.5.cloned.1.call-start = ((), (), s32[]{:S(2)}) async-start(), calls=%async_computation.9 | async-start | bytes 15728640 | tf_op jit(solution)/shard_map/reduce_scatter | solution.py:97
  153.7 7.8 %copy-start.6 = (bf16[1,2048,512]{2,1,0:T(8,128)(2,1)S(1)}, bf16[1,2048,512]{2,1,0:T(8,128)(2,1)}, u32[]{:S(2)}) copy-start(bf16[1,2048,512]{2,1,0:T(8,128)(2,1)} %param.11) | copy-start | bytes 6291460
  153.7 7.8 %copy-start.12 = (bf16[1280,2048]{1,0:T(8,128)(2,1)S(1)}, bf16[1280,2048]{1,0:T(8,128)(2,1)}, u32[]{:S(2)}) copy-start(bf16[1280,2048]{1,0:T(8,128)(2,1)} %all-gather.5.cloned.1.call-done) | copy-start | bytes 15728644
  225.7 3.2 copy-start.13
  225.7 3.2 copy-start.7
  356.6 7.0 %copy-start.14 = (bf16[1280,512]{0,1:T(8,128)(2,1)S(1)}, bf16[1280,512]{0,1:T(8,128)(2,1)}, u32[]{:S(2)}) copy-start(bf16[1280,512]{0,1:T(8,128)(2,1)} %copy-done.13) | copy-start | bytes 3932164
  356.6 127.9 %all-to-all-start.3 = ((f32[16,80,1024]{2,1,0:T(8,128)}), f32[16,80,1024]{2,1,0:T(8,128)}, u32[]{:S(2)}, u32[]{:S(2)}) async-start(f32[16,80,1024]{2,1,0:T(8,128)} %bitcast.88), calls=%async_computation.4 | async-start | bytes 10485760 | tf_op jit(solution)/shard_map/all_to_all | solution.py:100
  363.3 107.4 %reduce-scatter.7.cloned.1.call-start = ((), (), s32[]{:S(2)}) async-start(), calls=%async_computation.10 | async-start | bytes 1114112
  363.6 14.5 %slice-start = ((s8[5242880]{0:T(1024)(128)(4,1)}), s8[4194304]{0:T(1024)(128)(4,1)S(1)}, s32[]{:S(2)}) async-start(s8[5242880]{0:T(1024)(128)(4,1)} %bitcast.96), calls=%async_computation.11 | async-start | bytes 8388608
  370.9 7.2 %slice-start.1 = ((s8[5242880]{0:T(1024)(128)(4,1)}), s8[1048576]{0:T(1024)(128)(4,1)S(1)}, s32[]{:S(2)}) async-start(s8[5242880]{0:T(1024)(128)(4,1)} %bitcast.96), calls=%async_computation.12 | async-start | bytes 2097152
  370.9 7.2 %copy-start.15 = (bf16[1280,512]{0,1:T(8,128)(2,1)S(1)}, bf16[1280,512]{0,1:T(8,128)(2,1)}, u32[]{:S(2)}) copy-start(bf16[1280,512]{0,1:T(8,128)(2,1)} %get-tuple-element.9) | copy-start | bytes 3932164
  378.1 5.0 %copy-start.3 = (bf16[128,2048]{1,0:T(8,128)(2,1)S(1)}, bf16[128,2048]{1,0:T(8,128)(2,1)}, u32[]{:S(2)}) copy-start(bf16[128,2048]{1,0:T(8,128)(2,1)} %param.7) | copy-start | bytes 1572868
  383.1 104.8 %copy-start.11 = (f32[128,2]{0,1:T(2,128)}, f32[128,2]{0,1:T(2,128)S(1)}, u32[]{:S(2)}) copy-start(f32[128,2]{0,1:T(2,128)S(1)} %copy.70) | copy-start | bytes 3076
  472.2 15.8 %copy-start.5 = (f32[320,128]{1,0:T(8,128)S(1)}, f32[320,128]{1,0:T(8,128)}, u32[]{:S(2)}) copy-start(f32[320,128]{1,0:T(8,128)} %copy-done.4) | copy-start | bytes 491524
  484.6 5.2 %copy-start.1 = (bf16[1,2048,512]{2,1,0:T(8,128)(2,1)S(1)}, bf16[1,2048,512]{2,1,0:T(8,128)(2,1)}, u32[]{:S(2)}) copy-start(bf16[1,2048,512]{2,1,0:T(8,128)(2,1)} %param.10) | copy-start | bytes 6291460
Sparse Core Ops, SparseCore 0:
  77.8 68.0 all-gather.4
  147.5 68.5 all-gather.2
  234.7 121.9 reduce-scatter.4
  385.0 85.6 reduce-scatter.6
where the time goes:
time: 497 us; the launch traced here: 496 us
  waiting for transfers between devices  255 us (51%)
  blocking collectives  152 us (31%)
  matrix products  54.4 us (11%)
  between operations  14.1 us (3%)
  local copies, waits for them, and re-layouts  8.03 us (2%)
  starting transfers between devices  6.8 us (1%)
  other arithmetic  6.04 us (1%)
    reduce_scatter x1, waiting for transfers between devices, shards(): lax.psum_scatter(row_grad, 'tp', scatter_dimension=1, tiled=True)  107 us
    unnamed x5, waiting for transfers between devices  85.4 us
    all_to_all x1, blocking collectives, shards(): lax.all_to_all(tok_send, 'ep', split_axis=0, concat_axis=0, tiled=True)  64.9 us
    all_to_all x1, blocking collectives, shards(): lax.all_to_all(cot_send, 'ep', split_axis=0, concat_axis=0, tiled=True)  63.8 us
    all_gather x1, waiting for transfers between devices, shards(): lax.all_gather(cot_half, 'tp', axis=1, tiled=True)  49.9 us
    all_to_all x1, waiting for transfers between devices, shards(): lax.all_to_all(row_share, 'ep', split_axis=0, concat_axis=0, tiled=True)  12.4 us
    all_to_all x1, blocking collectives, shards(): lax.all_to_all(gate_total, 'ep', split_axis=0, concat_axis=0, tiled=True)  11.4 us
  transfers between devices with their start and end apart: 5, of which 4 were waited for; matrix products, arithmetic and copies ran while one was open for 8% of the time, Pallas kernels for 0%

commit v1 on v0

--- a/solution.py
+++ b/solution.py
@@ -60,7 +60,9 @@
     )
     tok_rows, cot_rows = (
         lax.all_gather(tok_half, "tp", axis=1, tiled=True),
-        lax.all_gather(cot_half, "tp", axis=1, tiled=True),
+        jnp.concatenate(
+            lax.all_to_all(jnp.stack([cot_half] * lax.axis_size("tp")), "tp", 0, 0), axis=1
+        ),
     )
     w_gate = gate_proj[0]
     w_up = up_proj[0]

time: 497 us -> 513 us (1.032)
  blocking collectives: 152 us -> 15.6 us
  waiting for transfers between devices: 255 us -> 378 us
  starting transfers between devices: 6.8 us -> 28.5 us
  local copies, waits for them, and re-layouts: 8.03 us -> 18 us
  matrix products: 54.4 us -> 46.9 us
  other arithmetic: 6.04 us -> 11.4 us
    all_to_all x0 -> x4, waiting for transfers between devices: none -> 173 us  [the longest x1 58.4 us: shards(): lax.all_to_all(tok_send, 'ep', split_axis=0, concat_axis=0, tiled=True)]
    all_to_all x3 -> x0, blocking collectives: 137 us -> none  [the longest x1 64.9 us: shards(): lax.all_to_all(tok_send, 'ep', split_axis=0, concat_axis=0, tiled=True)]
    all_gather x1 -> x0, waiting for transfers between devices: 49.9 us -> none  [shards(): lax.all_gather(cot_half, 'tp', axis=1, tiled=True)]
    all_to_all x0 -> x4, starting transfers between devices: none -> 21.9 us  [the longest x1 6.65 us: shards(): lax.all_to_all(tok_send, 'ep', split_axis=0, concat_axis=0, tiled=True)]
    reshape x0 -> x1, local copies, waits for them, and re-layouts: none -> 7.96 us  [shards(): jnp.concatenate(lax.all_to_all(jnp.stack([cot_half] * lax.axis_size('tp')...]
    another operation x4 -> x5, other arithmetic: 1.28 us -> 6.59 us  [the longest x1 5.31 us: shards(): jnp.stack([cot_half] * lax.axis_size('tp'))]
    unnamed x5 -> x4, waiting for transfers between devices: 85.4 us -> 85.6 us
  transfers between devices with their start and end apart: 5 -> 8, of which waited for: 4 -> 6; matrix products, arithmetic and copies ran while one was open for 8% -> 8% of each run, Pallas kernels for 0% -> 0%
where the time goes in v1:
time: 513 us; the launch traced here: 512 us
  waiting for transfers between devices  378 us (74%)
  matrix products  46.9 us (9%)
  starting transfers between devices  28.5 us (6%)
  local copies, waits for them, and re-layouts  18 us (4%)
  blocking collectives  15.6 us (3%)
  between operations  14.1 us (3%)
  other arithmetic  11.4 us (2%)
    reduce_scatter x1, waiting for transfers between devices, shards(): lax.psum_scatter(row_grad, 'tp', scatter_dimension=1, tiled=True)  107 us
    unnamed x4, waiting for transfers between devices  85.6 us
    all_to_all x1, waiting for transfers between devices, shards(): lax.all_to_all(tok_send, 'ep', split_axis=0, concat_axis=0, tiled=True)  58.4 us
    all_to_all x1, waiting for transfers between devices, shards(): lax.all_to_all(jnp.stack([cot_half] * lax.axis_size('tp')), 'tp', 0, 0)  58.2 us
    all_to_all x1, waiting for transfers between devices, shards(): lax.all_to_all(cot_send, 'ep', split_axis=0, concat_axis=0, tiled=True)  56.5 us
    all_to_all x1, waiting for transfers between devices, shards(): lax.all_to_all(row_share, 'ep', split_axis=0, concat_axis=0, tiled=True)  12.2 us
    all_to_all x1, blocking collectives, shards(): lax.all_to_all(gate_total, 'ep', split_axis=0, concat_axis=0, tiled=True)  11.7 us
  transfers between devices with their start and end apart: 8, of which 6 were waited for; matrix products, arithmetic and copies ran while one was open for 8% of the time, Pallas kernels for 0%

profile of v1, /device:TPU:11, one launch (start us, length us, event | category | flops | bytes accessed | tf_op | source)
XLA Modules:
  0.0 512.0 jit_solution(17560177971899138219)
XLA Ops:
  14.2 6.7 %all-to-all-start.3 = ((bf16[16,80,1024]{2,1,0:T(8,128)(2,1)}), bf16[16,80,1024]{2,1,0:T(8,128)(2,1)}, u32[]{:S(2)}, u32[]{:S(2)}) async-start(bf16[16,80,1024]{2,1,0:T(8,128)(2,1)} %bitcast.87), calls=%async_computation.3 | async-start | bytes 5242880 | tf_op jit(solution)/shard_map/all_to_all | solution.py:57
  21.2 58.4 %all-to-all-done.3 = bf16[16,80,1024]{2,1,0:T(8,128)(2,1)} async-done(((bf16[16,80,1024]{2,1,0:T(8,128)(2,1)}), bf16[16,80,1024]{2,1,0:T(8,128)(2,1)}, u32[]{:S(2)}, u32[]{:S(2)}) %all-to-all-start.3) | async-done | bytes 2621472 | tf_op jit(solution)/shard_map/all_to_all | solution.py:57
  81.4 4.8 all-to-all-start.1
  88.8 56.5 %all-to-all-done.1 = bf16[16,80,1024]{2,1,0:T(8,128)(2,1)} async-done(((bf16[16,80,1024]{2,1,0:T(8,128)(2,1)}), bf16[16,80,1024]{2,1,0:T(8,128)(2,1)}, u32[]{:S(2)}, u32[]{:S(2)}) %all-to-all-start.1) | async-done | bytes 2621472 | tf_op jit(solution)/shard_map/all_to_all | solution.py:58
  145.3 4.5 all-to-all-start
  149.8 5.3 %pad_maximum_fusion = bf16[2,1280,1024]{2,1,0:T(8,128)(2,1)} fusion(bf16[1,1280,1024]{2,1,0:T(8,128)(2,1)} %bitcast.6), kind=kLoop, calls=%fused_computation.1 | loop fusion | flops 2621440 | bytes 7864320 | tf_op jit(solution)/shard_map/stack | solution.py:64
  155.1 5.9 %all-to-all-start.2 = ((bf16[2,1280,1024]{2,1,0:T(8,128)(2,1)}), bf16[2,1280,1024]{2,1,0:T(8,128)(2,1)}, u32[]{:S(2)}, u32[]{:S(2)}) async-start(bf16[2,1280,1024]{2,1,0:T(8,128)(2,1)} %pad_maximum_fusion), calls=%async_computation.2 | async-start | bytes 10485760 | tf_op jit(solution)/shard_map/all_to_all | solution.py:64
  161.2 58.2 %all-to-all-done.2 = bf16[2,1280,1024]{2,1,0:T(8,128)(2,1)} async-done(((bf16[2,1280,1024]{2,1,0:T(8,128)(2,1)}), bf16[2,1280,1024]{2,1,0:T(8,128)(2,1)}, u32[]{:S(2)}, u32[]{:S(2)}) %all-to-all-start.2) | async-done | bytes 5242912 | tf_op jit(solution)/shard_map/all_to_all | solution.py:64
  219.3 8.0 %copy.79 = bf16[1280,2,1024]{0,2,1:T(8,128)(2,1)} copy(bf16[1280,2,1024]{2,0,1:T(8,128)(2,1)} %bitcast.7) | data formatting | bytes 10485760 | tf_op jit(solution)/shard_map/reshape | solution.py:63
  227.3 5.7 %fusion.5 = f32[1280,512]{0,1:T(8,128)S(1)} fusion(bf16[1280,2048]{1,0:T(8,128)(2,1)} %all-gather.2.cloned.1.call-done, bf16[1,2048,512]{2,1,0:T(8,128)(2,1)S(1)} %copy-done), kind=kOutput, calls=%fused_computation.18 | convolution fusion | flops 2684354560 | bytes 9961472 | tf_op jit(solution)/shard_map/dot_general | solution.py:70
  233.1 3.2 fusion.8
  236.3 5.0 fusion
  241.3 2.9 fusion.3
  244.3 5.8 %convolution_add_fusion = f32[1280,2048]{1,0:T(8,128)} fusion(f32[1280,2048]{1,0:T(8,128)S(1)} %fusion.3, bf16[1280,512]{0,1:T(8,128)(2,1)S(1)} %get-tuple-element.11, bf16[1,2048,512]{2,1,0:T(8,128)(2,1)S(1)} %copy-done.6), kind=kOutput, calls=%fused_computation | convolution fusion | flops 2686976000 | bytes 24379392 | tf_op jit(solution)/shard_map/dot_general | solution.py:96
  250.2 3.8 psum.7
  254.0 11.7 %all_to_all.53 = f32[16,80,1]{1,2,0:T(1,128)S(1)} all-to-all(f32[16,80,1]{1,2,0:T(1,128)S(1)} %bitcast.99), channel_id=1, replica_groups=mesh['ep'=16,'tp'=2] {'ep'}, dimensions={0} | all-to-all | bytes 10240 | tf_op jit(solution)/shard_map/all_to_all | solution.py:103
  265.7 106.8 %reduce-scatter.5.cloned.1.call-done = f32[1280,1024]{1,0:T(8,128)} async-done(((f32[1280,2048]{1,0:T(8,128)}), f32[1280,1024]{1,0:T(8,128)}) %reduce-scatter.5.cloned.1.call-update) | async-done | bytes 5242896 | tf_op jit(solution)/shard_map/reduce_scatter | solution.py:99
  372.6 6.5 %all-to-all-start.4 = ((f32[16,80,1024]{2,1,0:T(8,128)}), f32[16,80,1024]{2,1,0:T(8,128)}, u32[]{:S(2)}, u32[]{:S(2)}) async-start(f32[16,80,1024]{2,1,0:T(8,128)} %bitcast.88), calls=%async_computation.5 | async-start | bytes 10485760 | tf_op jit(solution)/shard_map/all_to_all | solution.py:102
  379.4 8.0 %convolution_bitcast_fusion.2 = f32[1,2048,512]{2,1,0:T(8,128)} fusion(bf16[1280,2048]{1,0:T(8,128)(2,1)} %all-gather.2.cloned.1.call-done, bf16[1280,512]{0,1:T(8,128)(2,1)} %copy-done.13), kind=kOutput, calls=%fused_computation.7 | convolution fusion | flops 2684354560 | bytes 10747904 | tf_op jit(solution)/shard_map/dot_general | solution.py:87
  387.4 7.2 %convolution_bitcast_fusion.1 = f32[1,2048,512]{2,1,0:T(8,128)} fusion(bf16[1280,2048]{1,0:T(8,128)(2,1)} %all-gather.2.cloned.1.call-done, bf16[1280,512]{0,1:T(8,128)(2,1)S(1)} %get-tuple-element.11), kind=kOutput, calls=%fused_computation.6 | convolution fusion | flops 2684354560 | bytes 10747904 | tf_op jit(solution)/shard_map/dot_general | solution.py:90
  394.6 4.5 convolution_bitcast_fusion
  401.8 84.9 %reduce-scatter.7.cloned.1.call-done = f32[128,4]{1,0:T(8,128)} async-done(((f32[2048,4]{1,0:T(8,128)}), f32[128,4]{1,0:T(8,128)}) %reduce-scatter.7.cloned.1.call-update) | async-done | bytes 2064
  488.2 12.2 %all-to-all-done.4 = f32[16,80,1024]{2,1,0:T(8,128)} async-done(((f32[16,80,1024]{2,1,0:T(8,128)}), f32[16,80,1024]{2,1,0:T(8,128)}, u32[]{:S(2)}, u32[]{:S(2)}) %all-to-all-start.4) | async-done | bytes 5242912 | tf_op jit(solution)/shard_map/all_to_all | solution.py:102
  500.4 3.3 bitcast_reduce_fusion
  (97 shorter events, 18.2 us)
Async XLA Ops:
  7.2 220.2 %copy-start = (bf16[1,2048,512]{2,1,0:T(8,128)(2,1)S(1)}, bf16[1,2048,512]{2,1,0:T(8,128)(2,1)}, u32[]{:S(2)}) copy-start(bf16[1,2048,512]{2,1,0:T(8,128)(2,1)} %param.10) | copy-start | bytes 6291460
  11.0 9.8 %copy-start.4 = (f32[320,128]{1,0:T(8,128)}, f32[320,128]{1,0:T(8,128)S(1)}, u32[]{:S(2)}) copy-start(f32[320,128]{1,0:T(8,128)S(1)} %convert_reduce_fusion) | copy-start | bytes 491524
  14.2 6.7 %copy-start.7 = (bf16[128,2048]{1,0:T(8,128)(2,1)S(1)}, bf16[128,2048]{1,0:T(8,128)(2,1)}, u32[]{:S(2)}) copy-start(bf16[128,2048]{1,0:T(8,128)(2,1)} %param.13) | copy-start | bytes 1572868
  14.2 65.4 %all-to-all-start.3 = ((bf16[16,80,1024]{2,1,0:T(8,128)(2,1)}), bf16[16,80,1024]{2,1,0:T(8,128)(2,1)}, u32[]{:S(2)}, u32[]{:S(2)}) async-start(bf16[16,80,1024]{2,1,0:T(8,128)(2,1)} %bitcast.87), calls=%async_computation.3 | async-start | bytes 5242880 | tf_op jit(solution)/shard_map/all_to_all | solution.py:57
  81.4 63.8 %all-to-all-start.1 = ((bf16[16,80,1024]{2,1,0:T(8,128)(2,1)}), bf16[16,80,1024]{2,1,0:T(8,128)(2,1)}, u32[]{:S(2)}, u32[]{:S(2)}) async-start(bf16[16,80,1024]{2,1,0:T(8,128)(2,1)} %bitcast.86), calls=%async_computation.1 | async-start | bytes 5242880 | tf_op jit(solution)/shard_map/all_to_all | solution.py:58
  86.3 141.1 %all-gather.2.cloned.1.call-start = ((), (), s32[]{:S(2)}) async-start(), calls=%async_computation.8 | async-start | bytes 7864320 | tf_op jit(solution)/shard_map/all_gather | solution.py:62
  145.3 9.8 %all-to-all-start = ((bf16[16,80,1]{1,2,0:T(2,128)(2,1)}), bf16[16,80,1]{1,2,0:T(2,128)(2,1)S(1)}, u32[]{:S(2)}, u32[]{:S(2)}) async-start(bf16[16,80,1]{1,2,0:T(2,128)(2,1)} %copy.78), calls=%async_computation | async-start | bytes 16384 | tf_op jit(solution)/shard_map/all_to_all | solution.py:59
  155.1 64.3 %all-to-all-start.2 = ((bf16[2,1280,1024]{2,1,0:T(8,128)(2,1)}), bf16[2,1280,1024]{2,1,0:T(8,128)(2,1)}, u32[]{:S(2)}, u32[]{:S(2)}) async-start(bf16[2,1280,1024]{2,1,0:T(8,128)(2,1)} %pad_maximum_fusion), calls=%async_computation.2 | async-start | bytes 10485760 | tf_op jit(solution)/shard_map/all_to_all | solution.py:64
  161.0 211.5 %reduce-scatter.5.cloned.1.call-start = ((), (), s32[]{:S(2)}) async-start(), calls=%async_computation.9 | async-start | bytes 15728640 | tf_op jit(solution)/shard_map/reduce_scatter | solution.py:99
  227.3 5.7 %copy-start.6 = (bf16[1,2048,512]{2,1,0:T(8,128)(2,1)S(1)}, bf16[1,2048,512]{2,1,0:T(8,128)(2,1)}, u32[]{:S(2)}) copy-start(bf16[1,2048,512]{2,1,0:T(8,128)(2,1)} %param.11) | copy-start | bytes 6291460
  227.3 5.7 %copy-start.11 = (bf16[1280,2048]{1,0:T(8,128)(2,1)S(1)}, bf16[1280,2048]{1,0:T(8,128)(2,1)}, u32[]{:S(2)}) copy-start(bf16[1280,2048]{1,0:T(8,128)(2,1)} %all-gather.2.cloned.1.call-done) | copy-start | bytes 15728644
  227.3 9.0 %slice-start = ((s8[5242880]{0:T(1024)(128)(4,1)}), s8[4194304]{0:T(1024)(128)(4,1)S(1)}, s32[]{:S(2)}) async-start(s8[5242880]{0:T(1024)(128)(4,1)} %bitcast.89), calls=%async_computation.11 | async-start | bytes 8388608
  233.1 3.2 slice-start.1
  233.1 3.2 copy-start.12
  241.3 2.9 copy-start.13
  372.6 127.8 %all-to-all-start.4 = ((f32[16,80,1024]{2,1,0:T(8,128)}), f32[16,80,1024]{2,1,0:T(8,128)}, u32[]{:S(2)}, u32[]{:S(2)}) async-start(f32[16,80,1024]{2,1,0:T(8,128)} %bitcast.88), calls=%async_computation.5 | async-start | bytes 10485760 | tf_op jit(solution)/shard_map/all_to_all | solution.py:102
  379.1 107.7 %reduce-scatter.7.cloned.1.call-start = ((), (), s32[]{:S(2)}) async-start(), calls=%async_computation.10 | async-start | bytes 1114112
  379.4 15.2 %slice-start.2 = ((s8[5242880]{0:T(1024)(128)(4,1)}), s8[4194304]{0:T(1024)(128)(4,1)S(1)}, s32[]{:S(2)}) async-start(s8[5242880]{0:T(1024)(128)(4,1)} %bitcast.92), calls=%async_computation.13 | async-start | bytes 8388608
  387.4 7.2 %slice-start.3 = ((s8[5242880]{0:T(1024)(128)(4,1)}), s8[1048576]{0:T(1024)(128)(4,1)S(1)}, s32[]{:S(2)}) async-start(s8[5242880]{0:T(1024)(128)(4,1)} %bitcast.92), calls=%async_computation.14 | async-start | bytes 2097152
  387.4 7.2 %copy-start.14 = (bf16[1280,512]{0,1:T(8,128)(2,1)S(1)}, bf16[1280,512]{0,1:T(8,128)(2,1)}, u32[]{:S(2)}) copy-start(bf16[1280,512]{0,1:T(8,128)(2,1)} %get-tuple-element.9) | copy-start | bytes 3932164
  394.6 5.0 copy-start.3
  399.6 104.1 %copy-start.10 = (f32[128,2]{0,1:T(2,128)}, f32[128,2]{0,1:T(2,128)S(1)}, u32[]{:S(2)}) copy-start(f32[128,2]{0,1:T(2,128)S(1)} %copy.85) | copy-start | bytes 3076
  488.2 15.5 %copy-start.5 = (f32[320,128]{1,0:T(8,128)S(1)}, f32[320,128]{1,0:T(8,128)}, u32[]{:S(2)}) copy-start(f32[320,128]{1,0:T(8,128)} %copy-done.4) | copy-start | bytes 491524
  500.4 5.1 %copy-start.1 = (bf16[1,2048,512]{2,1,0:T(8,128)(2,1)S(1)}, bf16[1,2048,512]{2,1,0:T(8,128)(2,1)}, u32[]{:S(2)}) copy-start(bf16[1,2048,512]{2,1,0:T(8,128)(2,1)} %param.10) | copy-start | bytes 6291460
  (3 other events, 3.3 us)
Sparse Core Ops, SparseCore 0:
  88.6 68.9 all-gather.1
  250.2 122.3 reduce-scatter.4
  401.5 85.1 reduce-scatter.6
